TPU v7x, 32 devices: a whole 2x2x4 slice. The times are simulated.
32 devices in a mesh: sp: 8 (over z, x), dp: 4 (over y, core).
Axes of the slice: x: 2, y: 2, z: 4, core: 2. Of those that a mesh axis runs over, the one named last changes fastest.
Arguments:
- lin_pre: bfloat16 [2048, 8192], P(None, ('dp', 'sp')), may hold values from -6 to 6
- gate_pre: bfloat16 [2048, 8192], P(None, ('dp', 'sp')), may hold values from -8 to 8
- w_depth: float32 [31, 2048], replicated, may hold values from -1 to 1
- ln_gain: float32 [2048], replicated, may hold values from 0.1 to 1.9
- ln_shift: float32 [2048], replicated, may hold values from -3 to 3
- w_out: bfloat16 [2048, 2048], P(None, 'dp'), may hold values from -0.125 to 0.125
Outputs:
- module_out: bfloat16 [8192, 2048], P(('dp', 'sp'))
All inputs are finite; a program needn't handle non-finite values.
Results may differ from a plain program's by a relative error of at most 0.0064.
Values may be sent and summed in bfloat16 or wider, within the bound.
A program may use at most 64 MiB of HBM per device.

v0:
```python
import jax
import jax.numpy as jnp
from jax import lax
from jax.sharding import PartitionSpec as P


def extended(cells, sides, width):
    for axis, dim in sides:
        count = lax.axis_size(axis)
        ends = count - 1
        head = lax.slice_in_dim(cells, 0, width, axis=dim)
        tail = lax.slice_in_dim(cells, cells.shape[dim] - width, cells.shape[dim], axis=dim)
        cells = jnp.concatenate(
            [
                lax.ppermute(tail, axis, [(i, (i + 1) % count) for i in range(ends)]),
                cells,
                lax.ppermute(head, axis, [((i + 1) % count, i) for i in range(ends)]),
            ],
            axis=dim,
        )
    return cells


def convolve(padded, kernel_taps, seq_span):
    running = jnp.zeros((padded.shape[0], seq_span), jnp.float32)
    for tap_index in range(kernel_taps.shape[0]):
        running = running + kernel_taps[tap_index][:, None] * padded[
            :, tap_index : tap_index + seq_span
        ].astype(jnp.float32)
    return running.astype(jnp.bfloat16)


def per_device(lin_pre, gate_pre, w_depth, ln_gain, ln_shift, w_out):
    glu = (lin_pre.astype(jnp.float32) * jax.nn.sigmoid(gate_pre.astype(jnp.float32))).astype(
        jnp.bfloat16
    )
    half_span = (w_depth.shape[0] - 1) // 2
    padded = extended(glu, (("sp", 1),), half_span)
    mixed = convolve(padded, w_depth, glu.shape[1])
    mixed_float = mixed.astype(jnp.float32)
    channel_mean = jnp.mean(mixed_float, axis=0, keepdims=True)
    variance = jnp.mean(jnp.square(mixed_float - channel_mean), axis=0, keepdims=True)
    normed = (mixed_float - channel_mean) * lax.rsqrt(variance + 1e-05)
    normed = normed * ln_gain[:, None] + ln_shift[:, None]
    activated = jax.nn.silu(normed).astype(jnp.bfloat16)
    product = lax.dot_general(
        activated,
        lax.all_gather(w_out, "dp", axis=1, tiled=True),
        (((0,), (0,)), ((), ())),
        preferred_element_type=jnp.float32,
    )
    return product.astype(jnp.bfloat16)


def solution(mesh):
    in_specs = (P(None, ("dp", "sp")), P(None, ("dp", "sp")), P(), P(), P(), P(None, "dp"))
    out_specs = P(("dp", "sp"), None)
    return jax.shard_map(
        per_device, mesh=mesh, in_specs=in_specs, out_specs=out_specs, check_vma=False
    )
```

profile of v0, /device:TPU:0, one launch (start us, length us, event | category | flops | bytes accessed | tf_op | source)
XLA Modules:
  0.0 83.7 jit_solution(12797835145404579786)
XLA Ops:
  6.5 0.0 copy-start.1
  6.5 0.0 copy-start
  6.5 0.0 all-gather.2.cloned.1.call-start
  6.5 0.7 all-gather.2.cloned.1.call-update
  7.3 0.5 copy-done.1
  7.8 0.3 copy-done
  8.1 0.0 copy-start.2
  8.1 0.6 multiply_convert_fusion
  8.6 0.2 fusion.46
  8.9 4.9 %collective-permute-start = (bf16[2048,15]{1,0:T(8,128)(2,1)S(1)}, bf16[2048,15]{1,0:T(8,128)(2,1)S(1)}, u32[]{:S(2)}, u32[]{:S(2)}) collective-permute-start(bf16[2048,15]{1,0:T(8,128)(2,1)S(1)} %get-tuple-element.7), channel_id=1, source_target_pairs={{0,4},{4,8},{8,12},{12,16},{16,20},{20,24},{24,28},{1,5},{5,9},{9,... | collective-permute-start | bytes 184328 | tf_op jit(solution)/shard_map/ppermute | solution.py:15
  13.8 1.3 %collective-permute-start.1 = (bf16[2048,15]{1,0:T(8,128)(2,1)S(1)}, bf16[2048,15]{1,0:T(8,128)(2,1)S(1)}, u32[]{:S(2)}, u32[]{:S(2)}) collective-permute-start(bf16[2048,15]{1,0:T(8,128)(2,1)S(1)} %get-tuple-element.8), channel_id=1, source_target_pairs={{4,0},{8,4},{12,8},{16,12},{20,16},{24,20},{28,24},{5,1},{9,5},{13... | collective-permute-start | bytes 184328 | tf_op jit(solution)/shard_map/ppermute | solution.py:17
  15.1 0.0 copy-done.2
  15.1 0.1 fusion.47
  15.2 0.1 fusion.48
  15.3 20.9 %collective-permute-done = bf16[2048,15]{1,0:T(8,128)(2,1)S(1)} collective-permute-done((bf16[2048,15]{1,0:T(8,128)(2,1)S(1)}, bf16[2048,15]{1,0:T(8,128)(2,1)S(1)}, u32[]{:S(2)}, u32[]{:S(2)}) %collective-permute-start) | collective-permute-done | bytes 61472 | tf_op jit(solution)/shard_map/ppermute | solution.py:15
  36.2 0.0 collective-permute-done.1
  36.2 0.0 copy-start.3
  36.2 0.0 copy-start.4
  36.2 25.4 %convert_reduce_fusion = (f32[256]{0:T(256)S(1)}, bf16[2048,256]{1,0:T(8,128)(2,1)S(1)}) fusion(bf16[2048,15]{1,0:T(8,128)(2,1)S(1)} %collective-permute-done.1, bf16[2048,256]{1,0:T(8,128)(2,1)S(1)} %multiply_convert_fusion, f32[2048]{0:T(1024)S(1)} %bitcast.61, f32[2048]{0:T(1024)S(1)} %bitcast.62, f32[2048]{0:T(1024)S(1)} %bitcast.33, ...), kind=kLoop, calls=%fused_computation.29 | loop fusion | flops 96993024 | bytes 2475008 | tf_op jit(solution)/shard_map/reduce_sum | solution.py:41
  61.6 0.3 fusion.2
  61.9 8.0 %all-gather.2.cloned.1.call-done = bf16[2048,2048]{1,0:T(8,128)(2,1)} async-done(((bf16[2048,512]{1,0:T(8,128)(2,1)}), bf16[2048,2048]{1,0:T(8,128)(2,1)}) %all-gather.2.cloned.1.call-update) | async-done | bytes 8388624 | tf_op jit(solution)/shard_map/all_gather | solution.py:48
  69.9 0.0 copy-done.3
  69.9 0.0 copy-done.4
  69.9 6.9 %convolution_convert_fusion = bf16[256,2048]{1,0:T(8,128)(2,1)} fusion(bf16[2048,2048]{1,0:T(8,128)(2,1)} %all-gather.2.cloned.1.call-done, bf16[2048,256]{1,0:T(8,128)(2,1)S(1)} %get-tuple-element.6, f32[2048]{0:T(1024)S(1)} %copy-done.3, f32[2048]{0:T(1024)S(1)} %copy-done.4, f32[256]{0:T(256)S(1)} %add_rsqrt_fusion, f32[256]{0:T(256)S(1)} %broadcast_multiply_fusion), kind=kOutput, calls=%fused_computation.30 | convolution fusion | flops 2153250816 | bytes 10504192 | tf_op jit(solution)/shard_map/dot_general | solution.py:46
  (2 shorter events, 0.0 us)
Async XLA Ops:
  6.5 1.2 %copy-start.1 = (bf16[2048,256]{1,0:T(8,128)(2,1)S(1)}, bf16[2048,256]{1,0:T(8,128)(2,1)}, u32[]{:S(2)}) copy-start(bf16[2048,256]{1,0:T(8,128)(2,1)} %param.6) | copy-start | bytes 3145732
  6.5 1.5 %copy-start = (bf16[2048,256]{1,0:T(8,128)(2,1)S(1)}, bf16[2048,256]{1,0:T(8,128)(2,1)}, u32[]{:S(2)}) copy-start(bf16[2048,256]{1,0:T(8,128)(2,1)} %param.7) | copy-start | bytes 3145732
  6.5 63.4 %all-gather.2.cloned.1.call-start = ((), (), s32[]{:S(2)}) async-start(), calls=%async_computation | async-start | bytes 10485760 | tf_op jit(solution)/shard_map/all_gather | solution.py:48
  8.1 7.0 %copy-start.2 = (f32[31,2048]{1,0:T(8,128)S(1)}, f32[31,2048]{1,0:T(8,128)}, u32[]{:S(2)}) copy-start(f32[31,2048]{1,0:T(8,128)} %param.8) | copy-start | bytes 761860
  8.9 27.3 %collective-permute-start = (bf16[2048,15]{1,0:T(8,128)(2,1)S(1)}, bf16[2048,15]{1,0:T(8,128)(2,1)S(1)}, u32[]{:S(2)}, u32[]{:S(2)}) collective-permute-start(bf16[2048,15]{1,0:T(8,128)(2,1)S(1)} %get-tuple-element.7), channel_id=1, source_target_pairs={{0,4},{4,8},{8,12},{12,16},{16,20},{20,24},{24,28},{1,5},{5,9},{9,... | collective-permute-start | bytes 184328 | tf_op jit(solution)/shard_map/ppermute | solution.py:15
  13.8 22.4 %collective-permute-start.1 = (bf16[2048,15]{1,0:T(8,128)(2,1)S(1)}, bf16[2048,15]{1,0:T(8,128)(2,1)S(1)}, u32[]{:S(2)}, u32[]{:S(2)}) collective-permute-start(bf16[2048,15]{1,0:T(8,128)(2,1)S(1)} %get-tuple-element.8), channel_id=1, source_target_pairs={{4,0},{8,4},{12,8},{16,12},{20,16},{24,20},{28,24},{5,1},{9,5},{13... | collective-permute-start | bytes 184328 | tf_op jit(solution)/shard_map/ppermute | solution.py:17
  36.2 33.7 %copy-start.3 = (f32[2048]{0:T(1024)S(1)}, f32[2048]{0:T(1024)}, u32[]{:S(2)}) copy-start(f32[2048]{0:T(1024)} %param.10) | copy-start | bytes 24580
  36.2 33.7 %copy-start.4 = (f32[2048]{0:T(1024)S(1)}, f32[2048]{0:T(1024)}, u32[]{:S(2)}) copy-start(f32[2048]{0:T(1024)} %param.9) | copy-start | bytes 24580
Sparse Core Ops, SparseCore 0:
  8.9 60.9 all-gather.1
where the time goes:
time: 83.9 us; the launch traced here: 83.7 us
  waiting for transfers between devices  29.5 us (35%)
  other arithmetic  26.3 us (31%)
  between operations  13.5 us (16%)
  matrix products  6.9 us (8%)
  starting transfers between devices  6.2 us (7%)
  local copies, waits for them, and re-layouts  1.26 us (2%)
    reduce_sum x1, other arithmetic, per_device(): channel_mean = jnp.mean(mixed_float, axis=0, keepdims=True)  25.4 us
    ppermute x1, waiting for transfers between devices, extended(): lax.ppermute(tail, axis, [(i, (i + 1) % count) for i in range(ends)])  20.9 us
    all_gather x1, waiting for transfers between devices, per_device(): lax.all_gather(w_out, 'dp', axis=1, tiled=True)  7.97 us
    dot_general x1, matrix products, per_device(): lax.dot_general(activated, lax.all_gather(w_out, 'dp', axis=1, tiled=True...  6.9 us
    ppermute x1, starting transfers between devices, extended(): lax.ppermute(tail, axis, [(i, (i + 1) % count) for i in range(ends)])  4.9 us
  transfers between devices with their start and end apart: 3, of which 2 were waited for; matrix products, arithmetic and copies ran while one was open for 32% of the time, Pallas kernels for 0%

commit v1 on v0

v1 whole, which is shorter than its diff:
```python
import functools

import jax
import jax.numpy as jnp
from jax import lax
from jax.experimental import pallas as pl
from jax.experimental.pallas import tpu as pltpu
from jax.sharding import PartitionSpec as P

MESH = pl.DeviceIdType.MESH
LANES = 128
PAD = 16
CHUNKS = 4


def kernel(
    n_sp, n_dp, lin_hbm, gate_hbm, taps, gain, shift, w_hbm, out,
    lin_v, gate_v, gpad, mixed, act, wbuf, stat,
    in_sem, own_sem, own_d2d, halo_send, halo_recv,
    y_send, y_recv, x_send, x_recv, z_send, z_recv, d_send, d_recv,
):
    channels, span = lin_hbm.shape
    taps_n = taps.shape[0]
    half = (taps_n - 1) // 2
    width = w_hbm.shape[1]
    slabs = channels // LANES
    s = lax.axis_index("sp")
    d = lax.axis_index("dp")
    g, core = d // 2, d % 2
    groups = n_dp // 2
    partner = (s, g * 2 + 1 - core)
    flip1 = s + 1 - 2 * (s % 2)
    hi = (s // 2) % 2
    flip2 = s + 2 - 4 * hi
    q = s % 4
    q1 = q + 1 - 2 * (s % 2)
    q2 = q + 2 - 4 * hi
    q3 = 3 - q
    piece = channels // 4
    rows = piece // CHUNKS
    n_b = CHUNKS // 4

    in_rows = channels // 4
    loads = []
    for i in range(4):
        for a, (src, dst) in enumerate(((gate_hbm, gate_v), (lin_hbm, lin_v))):
            cut = pl.ds(i * in_rows, in_rows)
            loads.append(pltpu.make_async_copy(src.at[cut, :], dst.at[cut, :], in_sem.at[a, i]))
            loads[-1].start()

    barrier = pltpu.get_barrier_semaphore()
    peers = [partner, (flip1, d), (flip2, d)]
    for k in range(1, groups):
        peers.append((s, ((g + k) % groups) * 2 + core))
    peers += [(lax.rem(s + 1, n_sp), d), (lax.rem(s + n_sp - 1, n_sp), d)]
    for peer in peers:
        pl.semaphore_signal(barrier, inc=1, device_id=peer, device_id_type=MESH)
    pl.semaphore_wait(barrier, len(peers))
    has_left, has_right = s > 0, s < n_sp - 1

    sends = []

    def at(block, p, i):
        start = pl.multiple_of(p * piece + i * rows, rows)
        return wbuf.at[block, pl.ds(start, rows), :]

    def own(p, i):
        start = pl.multiple_of(p * piece + i * rows, rows)
        return w_hbm.at[pl.ds(start, rows), :]

    def copy(src, dst, send, recv, device):
        return pltpu.make_async_remote_copy(
            src_ref=src, dst_ref=dst, send_sem=send, recv_sem=recv,
            device_id=device, device_id_type=MESH,
        )

    def push(*args):
        c = copy(*args)
        c.start()
        sends.append(c)

    n_a = CHUNKS - 2 * n_b
    b_part = list(range(0, n_b))
    c_part = list(range(n_b, 2 * n_b))
    a_part = list(range(2 * n_b, CHUNKS))
    for k in range(1, groups):
        target = (s, ((g + k) % groups) * 2 + core)
        for i in range(CHUNKS):
            push(own(q, i), at(d, q, i), y_send.at[k - 1, i], y_recv.at[k - 1, i], target)
        for n, i in enumerate(a_part):
            m = CHUNKS + n
            push(own(q3, i), at(d, q3, i), y_send.at[k - 1, m], y_recv.at[k - 1, m], target)
    push(w_hbm, wbuf.at[d], own_d2d.at[0], own_d2d.at[1], partner)
    own_copy = pltpu.make_async_copy(w_hbm, wbuf.at[d], own_sem)
    own_copy.start()

    def landed(block, p, i, send, recv):
        ref = at(block, p, i)
        copy(ref, ref, send, recv, partner).wait_recv()
        return ref

    def to_partner(ref, k, m):
        push(ref, ref, d_send.at[k - 1, m], d_recv.at[k - 1, m], partner)

    events = []

    def event(kind, k, i):
        def run():
            block = ((g + groups - k) % groups) * 2 + core
            if kind == "y":
                ref = landed(block, q, i, y_send.at[k - 1, i], y_recv.at[k - 1, i])
                push(ref, ref, x_send.at[k - 1, i], x_recv.at[k - 1, i], (flip1, d))
                push(ref, ref, z_send.at[k - 1, i], z_recv.at[k - 1, i], (flip2, d))
                to_partner(ref, k, i)
            elif kind == "x":
                ref = landed(block, q1, i, x_send.at[k - 1, i], x_recv.at[k - 1, i])
                if i in c_part:
                    m = CHUNKS + i - n_b
                    push(ref, ref, z_send.at[k - 1, m], z_recv.at[k - 1, m], (flip2, d))
                to_partner(ref, k, CHUNKS + i)
            elif kind == "z":
                ref = landed(block, q2, i, z_send.at[k - 1, i], z_recv.at[k - 1, i])
                if i in b_part:
                    m = CHUNKS + i
                    push(ref, ref, x_send.at[k - 1, m], x_recv.at[k - 1, m], (flip1, d))
                to_partner(ref, k, 2 * CHUNKS + i)
            elif kind == "yd":
                m = CHUNKS + i - 2 * n_b
                ref = landed(block, q3, i, y_send.at[k - 1, m], y_recv.at[k - 1, m])
                to_partner(ref, k, 3 * CHUNKS + i)
            elif kind == "xd":
                m = CHUNKS + i
                ref = landed(block, q3, i, x_send.at[k - 1, m], x_recv.at[k - 1, m])
                to_partner(ref, k, 3 * CHUNKS + i)
            else:
                m = CHUNKS + i - n_b
                ref = landed(block, q3, i, z_send.at[k - 1, m], z_recv.at[k - 1, m])
                to_partner(ref, k, 3 * CHUNKS + i)

        return run

    for k in range(1, groups):
        for i in range(CHUNKS + 1):
            if i < CHUNKS:
                events.append(event("y", k, i))
            if i > 0:
                events.append(event("x", k, i - 1))
                events.append(event("z", k, i - 1))
        for i in a_part[:-1]:
            events.append(event("yd", k, i))
        for i in b_part:
            events.append(event("xd", k, i))
        for i in c_part:
            events.append(event("zd", k, i))
        for i in a_part[-1:]:
            events.append(event("yd", k, i))

    def advance(count):
        for _ in range(min(count, len(events))):
            events.pop(0)()

    step = 2 * LANES
    eye = (
        lax.broadcasted_iota(jnp.int32, (span, span), 0)
        == lax.broadcasted_iota(jnp.int32, (span, span), 1)
    ).astype(jnp.float32).astype(jnp.bfloat16)

    @pl.when(jnp.logical_not(has_left))
    def _():
        gpad[:, 0:PAD, :] = jnp.zeros((slabs, PAD, LANES), jnp.float32)

    @pl.when(jnp.logical_not(has_right))
    def _():
        gpad[:, PAD + span :, :] = jnp.zeros((slabs, PAD, LANES), jnp.float32)

    for i in range(4):
        loads[2 * i].wait()
        loads[2 * i + 1].wait()
        per = in_rows // step

        def turn(n, carry):
            at_row = pl.multiple_of(n * step, step)
            cut = pl.ds(at_row, step)
            glu = (
                lin_v[cut, :].astype(jnp.float32)
                * jax.nn.sigmoid(gate_v[cut, :].astype(jnp.float32))
            ).astype(jnp.bfloat16)
            turned = lax.dot_general(
                eye, glu, (((1,), (1,)), ((), ())), preferred_element_type=jnp.float32
            )
            gpad[2 * n, pl.ds(PAD, span), :] = turned[:, :LANES]
            gpad[2 * n + 1, pl.ds(PAD, span), :] = turned[:, LANES:]
            return carry

        lax.fori_loop(i * per, (i + 1) * per, turn, 0)

    to_left = copy(
        gpad.at[:, pl.ds(PAD, PAD), :], gpad.at[:, pl.ds(PAD + span, PAD), :],
        halo_send.at[0], halo_recv.at[0], (s - 1, d),
    )
    to_right = copy(
        gpad.at[:, pl.ds(span, PAD), :], gpad.at[:, pl.ds(0, PAD), :],
        halo_send.at[1], halo_recv.at[1], (s + 1, d),
    )

    @pl.when(has_left)
    def _():
        to_left.start()

    @pl.when(has_right)
    def _():
        to_right.start()

    advance(1)

    @pl.when(has_left)
    def _():
        to_right.wait_recv()

    @pl.when(has_right)
    def _():
        to_left.wait_recv()

    tile = min(LANES, span)
    stat[0] = jnp.zeros((span, LANES), jnp.float32)

    def conv_slab(n, carry):
        lanes = pl.ds(pl.multiple_of(n * LANES, LANES), LANES)

        def tokens(t, inner):
            base = t * tile
            running = jnp.zeros((tile, LANES), jnp.float32)
            for j in range(taps_n):
                weight = taps[pl.ds(j, 1), lanes]
                running = running + weight * gpad[n, pl.ds(base + (PAD - half + j), tile), :]
            rounded = running.astype(jnp.bfloat16).astype(jnp.float32)
            at_token = pl.ds(pl.multiple_of(base, tile), tile)
            mixed[n, at_token, :] = rounded
            stat[0, at_token, :] += rounded
            return inner

        return lax.fori_loop(0, span // tile, tokens, carry)

    parts = 8
    for i in range(parts):
        lax.fori_loop(i * slabs // parts, (i + 1) * slabs // parts, conv_slab, 0)
        advance(2)

    mean = jnp.sum(stat[0], axis=1, keepdims=True) * (1.0 / channels)
    stat[0] = jnp.broadcast_to(mean, (span, LANES))
    stat[1] = jnp.zeros((span, LANES), jnp.float32)

    def spread(n, carry):
        apart = mixed[n] - stat[0]
        stat[1] += apart * apart
        return carry

    lax.fori_loop(0, slabs, spread, 0)
    variance = jnp.sum(stat[1], axis=1, keepdims=True) * (1.0 / channels)
    stat[1] = jnp.broadcast_to(lax.rsqrt(variance + 1e-05), (span, LANES))

    def activate(n, carry):
        lanes = pl.ds(pl.multiple_of(n * LANES, LANES), LANES)
        normed = (mixed[n] - stat[0]) * stat[1]
        normed = normed * gain[:, lanes] + shift[:, lanes]
        act[:, lanes] = (normed * jax.nn.sigmoid(normed)).astype(jnp.bfloat16)
        return carry

    lax.fori_loop(0, slabs, activate, 0)

    cols = min(width, 2 * LANES)

    def product(block):
        def columns(n, carry):
            at_col = pl.ds(pl.multiple_of(n * cols, cols), cols)
            at_out = pl.ds(pl.multiple_of(block * width + n * cols, cols), cols)
            out[:, at_out] = jnp.dot(
                act[...], wbuf[block, :, at_col], preferred_element_type=jnp.float32
            ).astype(out.dtype)
            return carry

        lax.fori_loop(0, width // cols, columns, 0)

    own_copy.wait()
    product(d)
    other = g * 2 + 1 - core
    copy(wbuf.at[other], wbuf.at[other], own_d2d.at[0], own_d2d.at[1], partner).wait_recv()
    product(other)
    advance(len(events))
    for k in range(1, groups):
        product(((g + groups - k) % groups) * 2 + core)
    for k in range(1, groups):
        block = ((g + groups - k) % groups) * 2 + 1 - core
        for p, at_piece in enumerate((q, q1, q2, q3)):
            for i in range(CHUNKS):
                m = p * CHUNKS + i
                landed(block, at_piece, i, d_send.at[k - 1, m], d_recv.at[k - 1, m])
        product(block)

    for c in sends:
        c.wait_send()

    @pl.when(has_left)
    def _():
        to_left.wait_send()

    @pl.when(has_right)
    def _():
        to_right.wait_send()


def solution(mesh):
    n_sp, n_dp = mesh.shape["sp"], mesh.shape["dp"]

    def per_device(lin_pre, gate_pre, w_depth, ln_gain, ln_shift, w_out):
        channels, span = lin_pre.shape
        width = w_out.shape[1]
        far = n_dp // 2 - 1
        n_b = CHUNKS // 4
        n_a = CHUNKS - 2 * n_b
        slabs = channels // LANES
        dma = pltpu.SemaphoreType.DMA
        vmem = pl.BlockSpec(memory_space=pltpu.VMEM)
        hbm = pl.BlockSpec(memory_space=pl.ANY)
        return pl.pallas_call(
            functools.partial(kernel, n_sp, n_dp),
            out_shape=jax.ShapeDtypeStruct((span, n_dp * width), jnp.bfloat16),
            in_specs=[hbm, hbm, vmem, vmem, vmem, hbm],
            out_specs=vmem,
            scratch_shapes=[
                pltpu.VMEM((channels, span), jnp.bfloat16),
                pltpu.VMEM((channels, span), jnp.bfloat16),
                pltpu.VMEM((slabs, span + 2 * PAD, LANES), jnp.float32),
                pltpu.VMEM((slabs, span, LANES), jnp.float32),
                pltpu.VMEM((span, channels), jnp.bfloat16),
                pltpu.VMEM((n_dp, channels, width), jnp.bfloat16),
                pltpu.VMEM((2, span, LANES), jnp.float32),
                dma((2, 4)),
                dma,
                dma((2,)),
                dma((2,)),
                dma((2,)),
                dma((far, CHUNKS + n_a)),
                dma((far, CHUNKS + n_a)),
                dma((far, CHUNKS + n_b)),
                dma((far, CHUNKS + n_b)),
                dma((far, CHUNKS + n_b)),
                dma((far, CHUNKS + n_b)),
                dma((far, 4 * CHUNKS)),
                dma((far, 4 * CHUNKS)),
            ],
            compiler_params=pltpu.CompilerParams(
                collective_id=0, has_side_effects=True, vmem_limit_bytes=60 * 2**20
            ),
            name="conv_module",
        )(lin_pre, gate_pre, w_depth, ln_gain[None, :], ln_shift[None, :], w_out)

    in_specs = (P(None, ("dp", "sp")), P(None, ("dp", "sp")), P(), P(), P(), P(None, "dp"))
    out_specs = P(("dp", "sp"), None)
    return jax.shard_map(
        per_device, mesh=mesh, in_specs=in_specs, out_specs=out_specs, check_vma=False
    )
```

time: 83.9 us -> 38.5 us (0.46)
  Pallas kernels: 0 us -> 36.1 us
  waiting for transfers between devices: 29.5 us -> 0 us
  other arithmetic: 26.3 us -> 0 us
  between operations: 13.5 us -> 0.01 us
  matrix products: 6.9 us -> 0 us
  starting transfers between devices: 6.2 us -> 0 us
  local copies, waits for them, and re-layouts: 1.26 us -> 2.3 us
    pallas_call x0 -> x1, Pallas kernels: none -> 36.1 us  [per_device(): pl.pallas_call(functools.partial(kernel, n_sp, n_dp), out_shape=jax.Shape...]
    reduce_sum x2 -> x0, other arithmetic: 25.7 us -> none  [the longest x1 25.4 us: per_device(): channel_mean = jnp.mean(mixed_float, axis=0, keepdims=True)]
    ppermute x2 -> x0, waiting for transfers between devices: 20.9 us -> none  [the longest x1 20.9 us: extended(): lax.ppermute(tail, axis, [(i, (i + 1) % count) for i in range(ends)])]
    all_gather x1 -> x0, waiting for transfers between devices: 7.97 us -> none  [per_device(): lax.all_gather(w_out, 'dp', axis=1, tiled=True)]
    dot_general x1 -> x0, matrix products: 6.9 us -> none  [per_device(): lax.dot_general(activated, lax.all_gather(w_out, 'dp', axis=1, tiled=True...]
    ppermute x2 -> x0, starting transfers between devices: 6.2 us -> none  [the longest x1 4.9 us: extended(): lax.ppermute(tail, axis, [(i, (i + 1) % count) for i in range(ends)])]
    unnamed x10 -> x1, local copies, waits for them, and re-layouts: 0.83 us -> 2.3 us
  transfers between devices with their start and end apart: 3 -> 0, of which waited for: 2 -> 0; matrix products, arithmetic and copies ran while one was open for 32% -> 0% of each run, Pallas kernels for 0% -> 0%
where the time goes in v1:
time: 38.5 us; the launch traced here: 38.4 us
  Pallas kernels  36.1 us (94%)
  local copies, waits for them, and re-layouts  2.3 us (6%)
    pallas_call x1, Pallas kernels, per_device(): pl.pallas_call(functools.partial(kernel, n_sp, n_dp), out_shape=jax.Shape...  36.1 us
    unnamed x1, local copies, waits for them, and re-layouts  2.3 us

profile of v1, /device:TPU:0, one launch (start us, length us, event | category | flops | bytes accessed | tf_op | source)
XLA Modules:
  0.0 38.4 jit_solution(18251809455331481758)
XLA Ops:
  0.0 36.1 %conv_module.1 = bf16[256,2048]{1,0:T(8,128)(2,1)} custom-call(bf16[2048,256]{1,0:T(8,128)(2,1)} %lin_hbm.1, bf16[2048,256]{1,0:T(8,128)(2,1)} %gate_hbm.1, f32[31,2048]{1,0:T(8,128)} %taps.1, f32[1,2048]{1,0:T(1,128)} %bitcast.2, f32[1,2048]{1,0:T(1,128)} %bitcast.3, bf16[2048,512]{1,0:T(8,128)(2,1)} %w_hbm.1), custom_call_target="tpu_custom_call" | custom-call | tf_op jit(solution)/shard_map/conv_module/pallas_call | solution.py:325
  36.1 2.3 %copy.8 = bf16[256,2048]{1,0:T(8,128)(2,1)} copy(bf16[256,2048]{1,0:T(8,128)(2,1)} %conv_module.1) | data formatting | bytes 2097152

commit v2 on v1

v2 whole, which is shorter than its diff:
```python
import functools

import jax
import jax.numpy as jnp
from jax import lax
from jax.experimental import pallas as pl
from jax.experimental.pallas import tpu as pltpu
from jax.sharding import PartitionSpec as P

MESH = pl.DeviceIdType.MESH
LANES = 128
PAD = 16
CHUNKS = 8
BY_X = 1
BY_Z = 2
BY_Y = CHUNKS - BY_X - BY_Z


def kernel(
    n_sp, n_dp, lin_hbm, gate_hbm, taps_hbm, gain_hbm, shift_hbm, w_hbm, out,
    lin_v, gate_v, taps, gain, shift, gpad, mixed, act, wbuf, stat, part, edge_out, edge_in,
    in_sem, small_sem, own_sem, own_d2d, halo_send, halo_recv,
    y_send, y_recv, x_send, x_recv, z_send, z_recv, d_send, d_recv,
):
    channels, span = lin_hbm.shape
    taps_n = taps.shape[0]
    half = (taps_n - 1) // 2
    width = w_hbm.shape[1]
    slabs = channels // LANES
    s = lax.axis_index("sp")
    d = lax.axis_index("dp")
    g, core = d // 2, d % 2
    groups = n_dp // 2
    partner = (s, g * 2 + 1 - core)
    other = g * 2 + 1 - core
    hi = (s // 2) % 2
    flip1 = s + 1 - 2 * (s % 2)
    flip2 = s + 2 - 4 * hi
    q = s % 4
    q1 = q + 1 - 2 * (s % 2)
    q2 = q + 2 - 4 * hi
    q3 = 3 - q
    piece = channels // 4
    rows = piece // CHUNKS

    barrier = pltpu.get_barrier_semaphore()
    peers = [partner, (flip1, d), (flip2, d)]
    for k in range(1, groups):
        peers.append((s, ((g + k) % groups) * 2 + core))
    peers += [(lax.rem(s + 1, n_sp), d), (lax.rem(s + n_sp - 1, n_sp), d)]
    for peer in peers:
        pl.semaphore_signal(barrier, inc=1, device_id=peer, device_id_type=MESH)
    has_left, has_right = s > 0, s < n_sp - 1

    def load(src, dst, sem):
        c = pltpu.make_async_copy(src, dst, sem)
        c.start()
        return c

    def piece_of(p):
        return pl.ds(pl.multiple_of(p * piece, piece), piece)

    def own_piece(n, p):
        return load(w_hbm.at[piece_of(p), :], wbuf.at[d, piece_of(p), :], own_sem.at[n])

    own_loads = [own_piece(0, q)]
    in_rows = channels // 4
    loads = []
    for i in range(4):
        cut = pl.ds(i * in_rows, in_rows)
        loads.append(load(gate_hbm.at[cut, :], gate_v.at[cut, :], in_sem.at[0, i]))
        loads.append(load(lin_hbm.at[cut, :], lin_v.at[cut, :], in_sem.at[1, i]))
    own_loads.append(own_piece(1, q3))
    small = [
        load(src, dst, small_sem.at[n])
        for n, (src, dst) in enumerate(((taps_hbm, taps), (gain_hbm, gain), (shift_hbm, shift)))
    ]
    own_loads.append(own_piece(2, q1))
    own_loads.append(own_piece(3, q2))

    sends = []

    def at(block, p, i):
        start = pl.multiple_of(p * piece + i * rows, rows)
        return wbuf.at[block, pl.ds(start, rows), :]

    def copy(src, dst, send, recv, device):
        return pltpu.make_async_remote_copy(
            src_ref=src, dst_ref=dst, send_sem=send, recv_sem=recv,
            device_id=device, device_id_type=MESH,
        )

    def push(*args):
        c = copy(*args)
        c.start()
        sends.append(c)

    own_loads[0].wait()
    pl.semaphore_wait(barrier, len(peers))

    b_part = list(range(0, BY_X))
    c_part = list(range(BY_X, BY_X + BY_Z))
    a_part = list(range(BY_X + BY_Z, CHUNKS))

    def send_y(p, i, m):
        for k in range(1, groups):
            target = (s, ((g + k) % groups) * 2 + core)
            push(at(d, p, i), at(d, p, i), y_send.at[k - 1, m], y_recv.at[k - 1, m], target)

    for i in range(CHUNKS):
        send_y(q, i, i)
    own_loads[1].wait()
    for n, i in enumerate(a_part):
        send_y(q3, i, CHUNKS + n)

    def landed(block, p, i, send, recv):
        ref = at(block, p, i)
        copy(ref, ref, send, recv, partner).wait_recv()
        return ref

    def to_partner(ref, k, m):
        push(ref, ref, d_send.at[k - 1, m], d_recv.at[k - 1, m], partner)

    def event(kind, k, i):
        def run():
            block = ((g + groups - k) % groups) * 2 + core
            if kind == "y":
                ref = landed(block, q, i, y_send.at[k - 1, i], y_recv.at[k - 1, i])
                push(ref, ref, x_send.at[k - 1, i], x_recv.at[k - 1, i], (flip1, d))
                push(ref, ref, z_send.at[k - 1, i], z_recv.at[k - 1, i], (flip2, d))
                to_partner(ref, k, i)
            elif kind == "x":
                ref = landed(block, q1, i, x_send.at[k - 1, i], x_recv.at[k - 1, i])
                if i in c_part:
                    m = CHUNKS + i - BY_X
                    push(ref, ref, z_send.at[k - 1, m], z_recv.at[k - 1, m], (flip2, d))
                to_partner(ref, k, CHUNKS + i)
            elif kind == "z":
                ref = landed(block, q2, i, z_send.at[k - 1, i], z_recv.at[k - 1, i])
                if i in b_part:
                    m = CHUNKS + i
                    push(ref, ref, x_send.at[k - 1, m], x_recv.at[k - 1, m], (flip1, d))
                to_partner(ref, k, 2 * CHUNKS + i)
            elif kind == "yd":
                m = CHUNKS + i - BY_X - BY_Z
                ref = landed(block, q3, i, y_send.at[k - 1, m], y_recv.at[k - 1, m])
                to_partner(ref, k, 3 * CHUNKS + i)
            elif kind == "xd":
                m = CHUNKS + i
                ref = landed(block, q3, i, x_send.at[k - 1, m], x_recv.at[k - 1, m])
                to_partner(ref, k, 3 * CHUNKS + i)
            else:
                m = CHUNKS + i - BY_X
                ref = landed(block, q3, i, z_send.at[k - 1, m], z_recv.at[k - 1, m])
                to_partner(ref, k, 3 * CHUNKS + i)

        return run

    plan = []
    for k in range(1, groups):
        for i in range(CHUNKS):
            plan.append((i + 1.0, event("y", k, i)))
            plan.append((i + 4.0, event("z", k, i)))
            plan.append((i + 4.5, event("x", k, i)))
        for n, i in enumerate(a_part):
            plan.append((CHUNKS + 1.0 + n, event("yd", k, i)))
        for n, i in enumerate(c_part):
            plan.append((CHUNKS + 4.0 + n, event("zd", k, i)))
        for n, i in enumerate(b_part):
            plan.append((CHUNKS + 4.5 + n, event("xd", k, i)))

    step = 2 * LANES
    eye = (
        lax.broadcasted_iota(jnp.int32, (span, span), 0)
        == lax.broadcasted_iota(jnp.int32, (span, span), 1)
    ).astype(jnp.float32).astype(jnp.bfloat16)

    for i in range(4):
        loads[2 * i].wait()
        loads[2 * i + 1].wait()
        per = in_rows // step

        def turn(n, carry):
            at_row = pl.multiple_of(n * step, step)
            cut = pl.ds(at_row, step)
            glu = (
                lin_v[cut, :].astype(jnp.float32)
                * jax.nn.sigmoid(gate_v[cut, :].astype(jnp.float32))
            ).astype(jnp.bfloat16)
            turned = lax.dot_general(
                eye, glu, (((1,), (1,)), ((), ())), preferred_element_type=jnp.float32
            )
            for m in range(2):
                slab = turned[:, m * LANES : (m + 1) * LANES]
                gpad[2 * n + m, pl.ds(PAD, span), :] = slab
                edge_out[0, 2 * n + m] = slab[:PAD].astype(jnp.bfloat16)
                edge_out[1, 2 * n + m] = slab[span - PAD :].astype(jnp.bfloat16)
            return carry

        lax.fori_loop(i * per, (i + 1) * per, turn, 0)

    to_left = copy(edge_out.at[0], edge_in.at[0], halo_send.at[0], halo_recv.at[0], (s - 1, d))
    to_right = copy(edge_out.at[1], edge_in.at[1], halo_send.at[1], halo_recv.at[1], (s + 1, d))

    @pl.when(has_left)
    def _():
        to_left.start()

    @pl.when(has_right)
    def _():
        to_right.start()

    for c in small:
        c.wait()
    stat[0] = jnp.zeros((span, LANES), jnp.float32)

    push(wbuf.at[d, piece_of(q), :], wbuf.at[d, piece_of(q), :], own_d2d.at[0, 0], own_d2d.at[1, 0], partner)
    push(wbuf.at[d, piece_of(q3), :], wbuf.at[d, piece_of(q3), :], own_d2d.at[0, 1], own_d2d.at[1, 1], partner)
    for n, p in ((2, q1), (3, q2)):
        own_loads[n].wait()
        push(wbuf.at[d, piece_of(p), :], wbuf.at[d, piece_of(p), :], own_d2d.at[0, n], own_d2d.at[1, n], partner)

    def halo():
        @pl.when(has_left)
        def _():
            to_right.wait_recv()
            gpad[:, 0:PAD, :] = edge_in[1].astype(jnp.float32)

        @pl.when(jnp.logical_not(has_left))
        def _():
            gpad[:, 0:PAD, :] = jnp.zeros((slabs, PAD, LANES), jnp.float32)

        @pl.when(has_right)
        def _():
            to_left.wait_recv()
            gpad[:, PAD + span :, :] = edge_in[0].astype(jnp.float32)

        @pl.when(jnp.logical_not(has_right))
        def _():
            gpad[:, PAD + span :, :] = jnp.zeros((slabs, PAD, LANES), jnp.float32)

    tile = min(LANES, span)

    def conv_slab(n, carry):
        lanes = pl.ds(pl.multiple_of(n * LANES, LANES), LANES)

        def tokens(t, inner):
            base = t * tile
            running = jnp.zeros((tile, LANES), jnp.float32)
            for j in range(taps_n):
                weight = taps[pl.ds(j, 1), lanes]
                running = running + weight * gpad[n, pl.ds(base + (PAD - half + j), tile), :]
            rounded = running.astype(jnp.bfloat16).astype(jnp.float32)
            at_token = pl.ds(pl.multiple_of(base, tile), tile)
            mixed[n, at_token, :] = rounded
            stat[0, at_token, :] += rounded
            return inner

        return lax.fori_loop(0, span // tile, tokens, carry)

    parts = 8

    def conv(i):
        return lambda: lax.fori_loop(i * slabs // parts, (i + 1) * slabs // parts, conv_slab, 0)

    def norm():
        mean = jnp.sum(stat[0], axis=1, keepdims=True) * (1.0 / channels)
        stat[0] = jnp.broadcast_to(mean, (span, LANES))
        stat[1] = jnp.zeros((span, LANES), jnp.float32)

        def spread(n, carry):
            apart = mixed[n] - stat[0]
            stat[1] += apart * apart
            return carry

        lax.fori_loop(0, slabs, spread, 0)
        variance = jnp.sum(stat[1], axis=1, keepdims=True) * (1.0 / channels)
        stat[1] = jnp.broadcast_to(lax.rsqrt(variance + 1e-05), (span, LANES))

    def activate():
        def one(n, carry):
            lanes = pl.ds(pl.multiple_of(n * LANES, LANES), LANES)
            normed = (mixed[n] - stat[0]) * stat[1]
            normed = normed * gain[:, lanes] + shift[:, lanes]
            act[:, lanes] = (normed * jax.nn.sigmoid(normed)).astype(jnp.bfloat16)
            return carry

        lax.fori_loop(0, slabs, one, 0)

    cols = min(width, 2 * LANES)

    def sweep(block, body):
        def columns(n, carry):
            at_col = pl.ds(pl.multiple_of(n * cols, cols), cols)
            at_out = pl.ds(pl.multiple_of(block * width + n * cols, cols), cols)
            body(at_col, at_out)
            return carry

        lax.fori_loop(0, width // cols, columns, 0)

    def product(block):
        def body(at_col, at_out):
            out[:, at_out] = jnp.dot(
                act[...], wbuf[block, :, at_col], preferred_element_type=jnp.float32
            ).astype(out.dtype)

        sweep(block, body)

    def slice_dot(block, p, at_col):
        return jnp.dot(
            act[:, piece_of(p)], wbuf[block, piece_of(p), at_col],
            preferred_element_type=jnp.float32,
        )

    def early(slot, block):
        def body(at_col, at_out):
            total = slice_dot(block, q, at_col) + slice_dot(block, q1, at_col)
            part[slot, :, at_col] = total + slice_dot(block, q2, at_col)

        sweep(block, body)

    def late(slot, block):
        def body(at_col, at_out):
            total = part[slot, :, at_col] + slice_dot(block, q3, at_col)
            out[:, at_out] = total.astype(out.dtype)

        sweep(block, body)

    def near(k):
        return ((g + groups - k) % groups) * 2 + core

    def far(k):
        return ((g + groups - k) % groups) * 2 + 1 - core

    def from_partner(k, n, p):
        for i in range(CHUNKS):
            m = n * CHUNKS + i
            landed(far(k), p, i, d_send.at[k - 1, m], d_recv.at[k - 1, m])

    def product_other():
        for n, p in enumerate((q, q3, q1, q2)):
            ref = wbuf.at[other, piece_of(p), :]
            copy(ref, ref, own_d2d.at[0, n], own_d2d.at[1, n], partner).wait_recv()
        product(other)

    def early_far(k):
        for n, p in enumerate((q, q1, q2)):
            from_partner(k, n, p)
        early(2 * k - 1, far(k))

    plan.append((3.6, halo))
    for i in range(parts):
        plan.append((4.6 + 0.75 * i, conv(i)))
    plan.append((10.7, norm))
    plan.append((11.2, activate))
    plan.append((11.7, lambda: product(d)))
    plan.append((12.2, product_other))
    for k in range(1, groups):
        plan.append((12.8, lambda k=k: early(2 * k - 2, near(k))))
        plan.append((13.1, lambda k=k: early_far(k)))
    for _, action in sorted(plan, key=lambda entry: entry[0]):
        action()
    for k in range(1, groups):
        late(2 * k - 2, near(k))
        from_partner(k, 3, q3)
        late(2 * k - 1, far(k))

    for c in sends:
        c.wait_send()

    @pl.when(has_left)
    def _():
        to_left.wait_send()

    @pl.when(has_right)
    def _():
        to_right.wait_send()


def solution(mesh):
    n_sp, n_dp = mesh.shape["sp"], mesh.shape["dp"]

    def per_device(lin_pre, gate_pre, w_depth, ln_gain, ln_shift, w_out):
        channels, span = lin_pre.shape
        width = w_out.shape[1]
        far = n_dp // 2 - 1
        slabs = channels // LANES
        dma = pltpu.SemaphoreType.DMA
        vmem = pl.BlockSpec(memory_space=pltpu.VMEM)
        hbm = pl.BlockSpec(memory_space=pl.ANY)
        return pl.pallas_call(
            functools.partial(kernel, n_sp, n_dp),
            out_shape=pltpu.VMEM((span, n_dp * width), jnp.bfloat16),
            in_specs=[hbm] * 6,
            out_specs=vmem,
            scratch_shapes=[
                pltpu.VMEM((channels, span), jnp.bfloat16),
                pltpu.VMEM((channels, span), jnp.bfloat16),
                pltpu.VMEM(w_depth.shape, jnp.float32),
                pltpu.VMEM((1, channels), jnp.float32),
                pltpu.VMEM((1, channels), jnp.float32),
                pltpu.VMEM((slabs, span + 2 * PAD, LANES), jnp.float32),
                pltpu.VMEM((slabs, span, LANES), jnp.float32),
                pltpu.VMEM((span, channels), jnp.bfloat16),
                pltpu.VMEM((n_dp, channels, width), jnp.bfloat16),
                pltpu.VMEM((2, span, LANES), jnp.float32),
                pltpu.VMEM((2 * far, span, width), jnp.float32),
                pltpu.VMEM((2, slabs, PAD, LANES), jnp.bfloat16),
                pltpu.VMEM((2, slabs, PAD, LANES), jnp.bfloat16),
                dma((2, 4)),
                dma((3,)),
                dma((4,)),
                dma((2, 4)),
                dma((2,)),
                dma((2,)),
                dma((far, CHUNKS + BY_Y)),
                dma((far, CHUNKS + BY_Y)),
                dma((far, CHUNKS + BY_X)),
                dma((far, CHUNKS + BY_X)),
                dma((far, CHUNKS + BY_Z)),
                dma((far, CHUNKS + BY_Z)),
                dma((far, 4 * CHUNKS)),
                dma((far, 4 * CHUNKS)),
            ],
            compiler_params=pltpu.CompilerParams(
                collective_id=0, has_side_effects=True, vmem_limit_bytes=60 * 2**20
            ),
            name="conv_module",
        )(lin_pre, gate_pre, w_depth, ln_gain[None, :], ln_shift[None, :], w_out)

    in_specs = (P(None, ("dp", "sp")), P(None, ("dp", "sp")), P(), P(), P(), P(None, "dp"))
    out_specs = P(("dp", "sp"), None)
    return jax.shard_map(
        per_device, mesh=mesh, in_specs=in_specs, out_specs=out_specs, check_vma=False
    )
```

time: 38.5 us -> 32.2 us (0.84)
  Pallas kernels: 36.1 us -> 31.1 us
  local copies, waits for them, and re-layouts: 2.3 us -> 0.97 us
    pallas_call x1, Pallas kernels: 36.1 us -> 31.1 us  [per_device(): pl.pallas_call(functools.partial(kernel, n_sp, n_dp), out_shape=pltpu.VME...]
    unnamed x1, local copies, waits for them, and re-layouts: 2.3 us -> 0.97 us
where the time goes in v2:
time: 32.2 us; the launch traced here: 32.1 us
  Pallas kernels  31.1 us (97%)
  local copies, waits for them, and re-layouts  0.97 us (3%)
    pallas_call x1, Pallas kernels, per_device(): pl.pallas_call(functools.partial(kernel, n_sp, n_dp), out_shape=pltpu.VME...  31.1 us
    unnamed x1, local copies, waits for them, and re-layouts  0.97 us

profile of v2, /device:TPU:0, one launch (start us, length us, event | category | flops | bytes accessed | tf_op | source)
XLA Modules:
  0.0 32.1 jit_solution(38061276752184315)
XLA Ops:
  0.0 31.1 %conv_module.1 = bf16[256,2048]{1,0:T(8,128)(2,1)S(1)} custom-call(bf16[2048,256]{1,0:T(8,128)(2,1)} %lin_hbm.1, bf16[2048,256]{1,0:T(8,128)(2,1)} %gate_hbm.1, f32[31,2048]{1,0:T(8,128)} %taps_hbm.1, f32[1,2048]{1,0:T(1,128)} %bitcast.2, f32[1,2048]{1,0:T(1,128)} %bitcast.3, bf16[2048,512]{1,0:T(8,128)(2,1)} %w_hbm.1), custom_call_target="tpu_custom_call" | custom-call | tf_op jit(solution)/shard_map/conv_module/pallas_call | solution.py:391
  31.1 1.0 %copy.8 = bf16[256,2048]{1,0:T(8,128)(2,1)} copy(bf16[256,2048]{1,0:T(8,128)(2,1)S(1)} %conv_module.1) | data formatting | bytes 2097152

commit v3 on v2

--- a/solution.py
+++ b/solution.py
@@ -10,9 +10,9 @@
 MESH = pl.DeviceIdType.MESH
 LANES = 128
 PAD = 16
-CHUNKS = 8
-BY_X = 1
-BY_Z = 2
+CHUNKS = 16
+BY_X = 3
+BY_Z = 4
 BY_Y = CHUNKS - BY_X - BY_Z
 
 
@@ -47,10 +47,19 @@
     peers = [partner, (flip1, d), (flip2, d)]
     for k in range(1, groups):
         peers.append((s, ((g + k) % groups) * 2 + core))
-    peers += [(lax.rem(s + 1, n_sp), d), (lax.rem(s + n_sp - 1, n_sp), d)]
     for peer in peers:
         pl.semaphore_signal(barrier, inc=1, device_id=peer, device_id_type=MESH)
     has_left, has_right = s > 0, s < n_sp - 1
+
+    @pl.when(has_left)
+    def _():
+        pl.semaphore_signal(barrier, inc=1, device_id=(s - 1, d), device_id_type=MESH)
+
+    @pl.when(has_right)
+    def _():
+        pl.semaphore_signal(barrier, inc=1, device_id=(s + 1, d), device_id_type=MESH)
+
+    n_peers = len(peers) + jnp.where(has_left, 1, 0) + jnp.where(has_right, 1, 0)
 
     def load(src, dst, sem):
         c = pltpu.make_async_copy(src, dst, sem)
@@ -78,8 +87,6 @@
     own_loads.append(own_piece(2, q1))
     own_loads.append(own_piece(3, q2))
 
-    sends = []
-
     def at(block, p, i):
         start = pl.multiple_of(p * piece + i * rows, rows)
         return wbuf.at[block, pl.ds(start, rows), :]
@@ -91,12 +98,10 @@
         )
 
     def push(*args):
-        c = copy(*args)
-        c.start()
-        sends.append(c)
+        copy(*args).start()
 
     own_loads[0].wait()
-    pl.semaphore_wait(barrier, len(peers))
+    pl.semaphore_wait(barrier, n_peers)
 
     b_part = list(range(0, BY_X))
     c_part = list(range(BY_X, BY_X + BY_Z))
@@ -105,7 +110,7 @@
     def send_y(p, i, m):
         for k in range(1, groups):
             target = (s, ((g + k) % groups) * 2 + core)
-            push(at(d, p, i), at(d, p, i), y_send.at[k - 1, m], y_recv.at[k - 1, m], target)
+            push(at(d, p, i), at(d, p, i), y_send.at[k - 1], y_recv.at[k - 1, m], target)
 
     for i in range(CHUNKS):
         send_y(q, i, i)
@@ -118,56 +123,59 @@
         copy(ref, ref, send, recv, partner).wait_recv()
         return ref
 
-    def to_partner(ref, k, m):
-        push(ref, ref, d_send.at[k - 1, m], d_recv.at[k - 1, m], partner)
+    def to_partner(ref, k, n):
+        push(ref, ref, d_send.at[k - 1], d_recv.at[k - 1, n], partner)
 
     def event(kind, k, i):
         def run():
             block = ((g + groups - k) % groups) * 2 + core
             if kind == "y":
-                ref = landed(block, q, i, y_send.at[k - 1, i], y_recv.at[k - 1, i])
-                push(ref, ref, x_send.at[k - 1, i], x_recv.at[k - 1, i], (flip1, d))
-                push(ref, ref, z_send.at[k - 1, i], z_recv.at[k - 1, i], (flip2, d))
-                to_partner(ref, k, i)
+                ref = landed(block, q, i, y_send.at[k - 1], y_recv.at[k - 1, i])
+                push(ref, ref, x_send.at[k - 1], x_recv.at[k - 1, i], (flip1, d))
+                push(ref, ref, z_send.at[k - 1], z_recv.at[k - 1, i], (flip2, d))
+                to_partner(ref, k, 0)
             elif kind == "x":
-                ref = landed(block, q1, i, x_send.at[k - 1, i], x_recv.at[k - 1, i])
+                ref = landed(block, q1, i, x_send.at[k - 1], x_recv.at[k - 1, i])
                 if i in c_part:
                     m = CHUNKS + i - BY_X
-                    push(ref, ref, z_send.at[k - 1, m], z_recv.at[k - 1, m], (flip2, d))
-                to_partner(ref, k, CHUNKS + i)
+                    push(ref, ref, z_send.at[k - 1], z_recv.at[k - 1, m], (flip2, d))
+                to_partner(ref, k, 0)
             elif kind == "z":
-                ref = landed(block, q2, i, z_send.at[k - 1, i], z_recv.at[k - 1, i])
+                ref = landed(block, q2, i, z_send.at[k - 1], z_recv.at[k - 1, i])
                 if i in b_part:
                     m = CHUNKS + i
-                    push(ref, ref, x_send.at[k - 1, m], x_recv.at[k - 1, m], (flip1, d))
-                to_partner(ref, k, 2 * CHUNKS + i)
+                    push(ref, ref, x_send.at[k - 1], x_recv.at[k - 1, m], (flip1, d))
+                to_partner(ref, k, 0)
             elif kind == "yd":
                 m = CHUNKS + i - BY_X - BY_Z
-                ref = landed(block, q3, i, y_send.at[k - 1, m], y_recv.at[k - 1, m])
-                to_partner(ref, k, 3 * CHUNKS + i)
+                ref = landed(block, q3, i, y_send.at[k - 1], y_recv.at[k - 1, m])
+                to_partner(ref, k, 1)
             elif kind == "xd":
                 m = CHUNKS + i
-                ref = landed(block, q3, i, x_send.at[k - 1, m], x_recv.at[k - 1, m])
-                to_partner(ref, k, 3 * CHUNKS + i)
+                ref = landed(block, q3, i, x_send.at[k - 1], x_recv.at[k - 1, m])
+                to_partner(ref, k, 1)
             else:
                 m = CHUNKS + i - BY_X
-                ref = landed(block, q3, i, z_send.at[k - 1, m], z_recv.at[k - 1, m])
-                to_partner(ref, k, 3 * CHUNKS + i)
+                ref = landed(block, q3, i, z_send.at[k - 1], z_recv.at[k - 1, m])
+                to_partner(ref, k, 1)
 
         return run
 
     plan = []
+    unit = 11.2 / CHUNKS
+    first_y, first_z, first_x = 1.9 + unit, 3.9 + 2 * unit, 4.4 + 2 * unit
     for k in range(1, groups):
         for i in range(CHUNKS):
-            plan.append((i + 1.0, event("y", k, i)))
-            plan.append((i + 4.0, event("z", k, i)))
-            plan.append((i + 4.5, event("x", k, i)))
+            plan.append((first_y + unit * i, event("y", k, i)))
+            later = 1.6 if unit * i < 8.4 else 0.6
+            plan.append((first_z + unit * i + later, event("z", k, i)))
+            plan.append((first_x + unit * i + later, event("x", k, i)))
         for n, i in enumerate(a_part):
-            plan.append((CHUNKS + 1.0 + n, event("yd", k, i)))
+            plan.append((first_y + unit * (CHUNKS + n), event("yd", k, i)))
         for n, i in enumerate(c_part):
-            plan.append((CHUNKS + 4.0 + n, event("zd", k, i)))
+            plan.append((first_z + unit * (CHUNKS + n), event("zd", k, i)))
         for n, i in enumerate(b_part):
-            plan.append((CHUNKS + 4.5 + n, event("xd", k, i)))
+            plan.append((first_x + unit * (CHUNKS + n), event("xd", k, i)))
 
     step = 2 * LANES
     eye = (
@@ -214,11 +222,9 @@
         c.wait()
     stat[0] = jnp.zeros((span, LANES), jnp.float32)
 
-    push(wbuf.at[d, piece_of(q), :], wbuf.at[d, piece_of(q), :], own_d2d.at[0, 0], own_d2d.at[1, 0], partner)
-    push(wbuf.at[d, piece_of(q3), :], wbuf.at[d, piece_of(q3), :], own_d2d.at[0, 1], own_d2d.at[1, 1], partner)
-    for n, p in ((2, q1), (3, q2)):
-        own_loads[n].wait()
-        push(wbuf.at[d, piece_of(p), :], wbuf.at[d, piece_of(p), :], own_d2d.at[0, n], own_d2d.at[1, n], partner)
+    own_loads[2].wait()
+    own_loads[3].wait()
+    push(wbuf.at[d], wbuf.at[d], own_d2d.at[0], own_d2d.at[1], partner)
 
     def halo():
         @pl.when(has_left)
@@ -239,24 +245,37 @@
         def _():
             gpad[:, PAD + span :, :] = jnp.zeros((slabs, PAD, LANES), jnp.float32)
 
-    tile = min(LANES, span)
+    def taps_sum(n, base, count):
+        lanes = pl.ds(pl.multiple_of(n * LANES, LANES), LANES)
+        running = jnp.zeros((count, LANES), jnp.float32)
+        for j in range(taps_n):
+            weight = taps[pl.ds(j, 1), lanes]
+            running = running + weight * gpad[n, pl.ds(base + (PAD - half + j), count), :]
+        rounded = running.astype(jnp.bfloat16).astype(jnp.float32)
+        at_token = pl.ds(pl.multiple_of(base, PAD), count)
+        mixed[n, at_token, :] = rounded
+        stat[0, at_token, :] += rounded
+
+    inner = span - 2 * PAD
+    tiles = next(m for m in range(2, inner) if inner % m == 0 and inner // m <= LANES and inner // m % PAD == 0)
+    tile = inner // tiles
 
     def conv_slab(n, carry):
-        lanes = pl.ds(pl.multiple_of(n * LANES, LANES), LANES)
-
-        def tokens(t, inner):
-            base = t * tile
-            running = jnp.zeros((tile, LANES), jnp.float32)
-            for j in range(taps_n):
-                weight = taps[pl.ds(j, 1), lanes]
-                running = running + weight * gpad[n, pl.ds(base + (PAD - half + j), tile), :]
-            rounded = running.astype(jnp.bfloat16).astype(jnp.float32)
-            at_token = pl.ds(pl.multiple_of(base, tile), tile)
-            mixed[n, at_token, :] = rounded
-            stat[0, at_token, :] += rounded
-            return inner
-
-        return lax.fori_loop(0, span // tile, tokens, carry)
+        def tokens(m, within):
+            taps_sum(n, PAD + m * tile, tile)
+            return within
+
+        return lax.fori_loop(0, tiles, tokens, carry)
+
+    def edges():
+        def one(n, carry):
+            def side(m, within):
+                taps_sum(n, m * (span - PAD), PAD)
+                return within
+
+            return lax.fori_loop(0, 2, side, carry, unroll=True)
+
+        lax.fori_loop(0, slabs, one, 0)
 
     parts = 8
 
@@ -277,7 +296,7 @@
         variance = jnp.sum(stat[1], axis=1, keepdims=True) * (1.0 / channels)
         stat[1] = jnp.broadcast_to(lax.rsqrt(variance + 1e-05), (span, LANES))
 
-    def activate():
+    def activate(h):
         def one(n, carry):
             lanes = pl.ds(pl.multiple_of(n * LANES, LANES), LANES)
             normed = (mixed[n] - stat[0]) * stat[1]
@@ -285,26 +304,28 @@
             act[:, lanes] = (normed * jax.nn.sigmoid(normed)).astype(jnp.bfloat16)
             return carry
 
-        lax.fori_loop(0, slabs, one, 0)
+        lax.fori_loop(h * slabs // 2, (h + 1) * slabs // 2, one, 0)
 
     cols = min(width, 2 * LANES)
 
-    def sweep(block, body):
+    halves = width // cols
+
+    def sweep(block, body, first=0, count=halves):
         def columns(n, carry):
             at_col = pl.ds(pl.multiple_of(n * cols, cols), cols)
             at_out = pl.ds(pl.multiple_of(block * width + n * cols, cols), cols)
             body(at_col, at_out)
             return carry
 
-        lax.fori_loop(0, width // cols, columns, 0)
-
-    def product(block):
+        lax.fori_loop(first, first + count, columns, 0)
+
+    def product(block, n):
         def body(at_col, at_out):
             out[:, at_out] = jnp.dot(
                 act[...], wbuf[block, :, at_col], preferred_element_type=jnp.float32
             ).astype(out.dtype)
 
-        sweep(block, body)
+        sweep(block, body, n, 1)
 
     def slice_dot(block, p, at_col):
         return jnp.dot(
@@ -332,41 +353,48 @@
     def far(k):
         return ((g + groups - k) % groups) * 2 + 1 - core
 
-    def from_partner(k, n, p):
-        for i in range(CHUNKS):
-            m = n * CHUNKS + i
-            landed(far(k), p, i, d_send.at[k - 1, m], d_recv.at[k - 1, m])
-
-    def product_other():
-        for n, p in enumerate((q, q3, q1, q2)):
-            ref = wbuf.at[other, piece_of(p), :]
-            copy(ref, ref, own_d2d.at[0, n], own_d2d.at[1, n], partner).wait_recv()
-        product(other)
+    def from_partner(k, n, size):
+        ref = wbuf.at[far(k), pl.ds(0, size * piece), :]
+        copy(ref, ref, d_send.at[k - 1], d_recv.at[k - 1, n], partner).wait_recv()
 
     def early_far(k):
-        for n, p in enumerate((q, q1, q2)):
-            from_partner(k, n, p)
+        from_partner(k, 0, 3)
         early(2 * k - 1, far(k))
 
-    plan.append((3.6, halo))
+    def take_other():
+        copy(wbuf.at[other], wbuf.at[other], own_d2d.at[0], own_d2d.at[1], partner).wait_recv()
+
     for i in range(parts):
-        plan.append((4.6 + 0.75 * i, conv(i)))
-    plan.append((10.7, norm))
-    plan.append((11.2, activate))
-    plan.append((11.7, lambda: product(d)))
-    plan.append((12.2, product_other))
+        plan.append((1.5 + 0.6 * i, conv(i)))
+    plan.append((6.3, halo))
+    plan.append((6.4, edges))
+    plan.append((7.3, norm))
+    plan.append((7.9, lambda: activate(0)))
+    plan.append((8.3, lambda: activate(1)))
+    for n in range(halves):
+        plan.append((8.7 + 1.0 * n / halves, lambda n=n: product(d, n)))
+        plan.append((9.8 + 1.0 * n / halves, lambda n=n: product(other, n)))
+    plan.append((9.75, take_other))
     for k in range(1, groups):
-        plan.append((12.8, lambda k=k: early(2 * k - 2, near(k))))
-        plan.append((13.1, lambda k=k: early_far(k)))
+        plan.append((first_x + unit * CHUNKS, lambda k=k: early(2 * k - 2, near(k))))
+        plan.append((first_x + unit * (CHUNKS + 1), lambda k=k: early_far(k)))
     for _, action in sorted(plan, key=lambda entry: entry[0]):
         action()
     for k in range(1, groups):
         late(2 * k - 2, near(k))
-        from_partner(k, 3, q3)
+        from_partner(k, 1, 1)
         late(2 * k - 1, far(k))
 
-    for c in sends:
-        c.wait_send()
+    def sent(sem, size):
+        ref = wbuf.at[d, pl.ds(0, size * rows), :]
+        copy(ref, ref, sem, own_d2d.at[1], partner).wait_send()
+
+    for k in range(1, groups):
+        sent(y_send.at[k - 1], CHUNKS + BY_Y)
+        sent(x_send.at[k - 1], CHUNKS + BY_X)
+        sent(z_send.at[k - 1], CHUNKS + BY_Z)
+        sent(d_send.at[k - 1], 4 * CHUNKS)
+    sent(own_d2d.at[0], 4 * CHUNKS)
 
     @pl.when(has_left)
     def _():
@@ -410,17 +438,17 @@
                 dma((2, 4)),
                 dma((3,)),
                 dma((4,)),
-                dma((2, 4)),
                 dma((2,)),
                 dma((2,)),
+                dma((2,)),
+                dma((far,)),
                 dma((far, CHUNKS + BY_Y)),
-                dma((far, CHUNKS + BY_Y)),
+                dma((far,)),
                 dma((far, CHUNKS + BY_X)),
-                dma((far, CHUNKS + BY_X)),
+                dma((far,)),
                 dma((far, CHUNKS + BY_Z)),
-                dma((far, CHUNKS + BY_Z)),
-                dma((far, 4 * CHUNKS)),
-                dma((far, 4 * CHUNKS)),
+                dma((far,)),
+                dma((far, 2)),
             ],
             compiler_params=pltpu.CompilerParams(
                 collective_id=0, has_side_effects=True, vmem_limit_bytes=60 * 2**20

time: 32.2 us -> 28.9 us (0.90)
  Pallas kernels: 31.1 us -> 27.8 us
    pallas_call x1, Pallas kernels: 31.1 us -> 27.8 us  [per_device(): pl.pallas_call(functools.partial(kernel, n_sp, n_dp), out_shape=pltpu.VME...]
where the time goes in v3:
time: 28.9 us; the launch traced here: 28.8 us
  Pallas kernels  27.8 us (96%)
  local copies, waits for them, and re-layouts  0.97 us (3%)
    pallas_call x1, Pallas kernels, per_device(): pl.pallas_call(functools.partial(kernel, n_sp, n_dp), out_shape=pltpu.VME...  27.8 us
    unnamed x1, local copies, waits for them, and re-layouts  0.97 us

profile of v3, /device:TPU:0, one launch (start us, length us, event | category | flops | bytes accessed | tf_op | source)
XLA Modules:
  0.0 28.8 jit_solution(6015825642756034088)
XLA Ops:
  0.0 27.8 %conv_module.1 = bf16[256,2048]{1,0:T(8,128)(2,1)S(1)} custom-call(bf16[2048,256]{1,0:T(8,128)(2,1)} %lin_hbm.1, bf16[2048,256]{1,0:T(8,128)(2,1)} %gate_hbm.1, f32[31,2048]{1,0:T(8,128)} %taps_hbm.1, f32[1,2048]{1,0:T(1,128)} %bitcast.2, f32[1,2048]{1,0:T(1,128)} %bitcast.3, bf16[2048,512]{1,0:T(8,128)(2,1)} %w_hbm.1), custom_call_target="tpu_custom_call" | custom-call | tf_op jit(solution)/shard_map/conv_module/pallas_call | solution.py:419
  27.8 1.0 %copy.8 = bf16[256,2048]{1,0:T(8,128)(2,1)} copy(bf16[256,2048]{1,0:T(8,128)(2,1)S(1)} %conv_module.1) | data formatting | bytes 2097152

commit v4 on v3

--- a/solution.py
+++ b/solution.py
@@ -11,9 +11,10 @@
 LANES = 128
 PAD = 16
 CHUNKS = 16
-BY_X = 3
-BY_Z = 4
+BY_X = 2
+BY_Z = 3
 BY_Y = CHUNKS - BY_X - BY_Z
+SOON = 3 * CHUNKS // 4
 
 
 def kernel(
@@ -139,25 +140,25 @@
                 if i in c_part:
                     m = CHUNKS + i - BY_X
                     push(ref, ref, z_send.at[k - 1], z_recv.at[k - 1, m], (flip2, d))
-                to_partner(ref, k, 0)
+                to_partner(ref, k, 1 if i < SOON else 2)
             elif kind == "z":
                 ref = landed(block, q2, i, z_send.at[k - 1], z_recv.at[k - 1, i])
                 if i in b_part:
                     m = CHUNKS + i
                     push(ref, ref, x_send.at[k - 1], x_recv.at[k - 1, m], (flip1, d))
-                to_partner(ref, k, 0)
+                to_partner(ref, k, 1 if i < SOON else 2)
             elif kind == "yd":
                 m = CHUNKS + i - BY_X - BY_Z
                 ref = landed(block, q3, i, y_send.at[k - 1], y_recv.at[k - 1, m])
-                to_partner(ref, k, 1)
+                to_partner(ref, k, 2)
             elif kind == "xd":
                 m = CHUNKS + i
                 ref = landed(block, q3, i, x_send.at[k - 1], x_recv.at[k - 1, m])
-                to_partner(ref, k, 1)
+                to_partner(ref, k, 2)
             else:
                 m = CHUNKS + i - BY_X
                 ref = landed(block, q3, i, z_send.at[k - 1], z_recv.at[k - 1, m])
-                to_partner(ref, k, 1)
+                to_partner(ref, k, 2)
 
         return run
 
@@ -167,7 +168,7 @@
     for k in range(1, groups):
         for i in range(CHUNKS):
             plan.append((first_y + unit * i, event("y", k, i)))
-            later = 1.6 if unit * i < 8.4 else 0.6
+            later = 1.0
             plan.append((first_z + unit * i + later, event("z", k, i)))
             plan.append((first_x + unit * i + later, event("x", k, i)))
         for n, i in enumerate(a_part):
@@ -327,23 +328,23 @@
 
         sweep(block, body, n, 1)
 
-    def slice_dot(block, p, at_col):
+    def slice_dot(block, p, at_col, low=0, high=CHUNKS):
+        at_row = pl.ds(pl.multiple_of(p * piece + low * rows, LANES), (high - low) * rows)
         return jnp.dot(
-            act[:, piece_of(p)], wbuf[block, piece_of(p), at_col],
-            preferred_element_type=jnp.float32,
+            act[:, at_row], wbuf[block, at_row, at_col], preferred_element_type=jnp.float32
         )
 
-    def early(slot, block):
+    def stage(which, slot, block):
         def body(at_col, at_out):
-            total = slice_dot(block, q, at_col) + slice_dot(block, q1, at_col)
-            part[slot, :, at_col] = total + slice_dot(block, q2, at_col)
-
-        sweep(block, body)
-
-    def late(slot, block):
-        def body(at_col, at_out):
-            total = part[slot, :, at_col] + slice_dot(block, q3, at_col)
-            out[:, at_out] = total.astype(out.dtype)
+            if which == 0:
+                part[slot, :, at_col] = slice_dot(block, q, at_col)
+            elif which == 1:
+                total = part[slot, :, at_col] + slice_dot(block, q1, at_col, 0, SOON)
+                part[slot, :, at_col] = total + slice_dot(block, q2, at_col, 0, SOON)
+            else:
+                total = part[slot, :, at_col] + slice_dot(block, q1, at_col, SOON)
+                total = total + slice_dot(block, q2, at_col, SOON)
+                out[:, at_out] = (total + slice_dot(block, q3, at_col)).astype(out.dtype)
 
         sweep(block, body)
 
@@ -353,13 +354,16 @@
     def far(k):
         return ((g + groups - k) % groups) * 2 + 1 - core
 
-    def from_partner(k, n, size):
-        ref = wbuf.at[far(k), pl.ds(0, size * piece), :]
-        copy(ref, ref, d_send.at[k - 1], d_recv.at[k - 1, n], partner).wait_recv()
-
-    def early_far(k):
-        from_partner(k, 0, 3)
-        early(2 * k - 1, far(k))
+    late = CHUNKS - SOON
+    shares = (CHUNKS, 2 * SOON, 2 * late + CHUNKS)
+
+    def stage_near(which, k):
+        stage(which, 2 * k - 2, near(k))
+
+    def stage_far(which, k):
+        ref = wbuf.at[far(k), pl.ds(0, shares[which] * rows), :]
+        copy(ref, ref, d_send.at[k - 1], d_recv.at[k - 1, which], partner).wait_recv()
+        stage(which, 2 * k - 1, far(k))
 
     def take_other():
         copy(wbuf.at[other], wbuf.at[other], own_d2d.at[0], own_d2d.at[1], partner).wait_recv()
@@ -376,14 +380,14 @@
         plan.append((9.8 + 1.0 * n / halves, lambda n=n: product(other, n)))
     plan.append((9.75, take_other))
     for k in range(1, groups):
-        plan.append((first_x + unit * CHUNKS, lambda k=k: early(2 * k - 2, near(k))))
-        plan.append((first_x + unit * (CHUNKS + 1), lambda k=k: early_far(k)))
+        for which, when in ((0, 13.2), (1, 14.6)):
+            plan.append((when, lambda k=k, which=which: stage_near(which, k)))
+            plan.append((when + 1.2, lambda k=k, which=which: stage_far(which, k)))
     for _, action in sorted(plan, key=lambda entry: entry[0]):
         action()
     for k in range(1, groups):
-        late(2 * k - 2, near(k))
-        from_partner(k, 1, 1)
-        late(2 * k - 1, far(k))
+        stage_near(2, k)
+        stage_far(2, k)
 
     def sent(sem, size):
         ref = wbuf.at[d, pl.ds(0, size * rows), :]
@@ -448,7 +452,7 @@
                 dma((far,)),
                 dma((far, CHUNKS + BY_Z)),
                 dma((far,)),
-                dma((far, 2)),
+                dma((far, 3)),
             ],
             compiler_params=pltpu.CompilerParams(
                 collective_id=0, has_side_effects=True, vmem_limit_bytes=60 * 2**20

time: 28.9 us -> 27.3 us (0.945)
  Pallas kernels: 27.8 us -> 26 us
    pallas_call x1, Pallas kernels: 27.8 us -> 26 us  [per_device(): pl.pallas_call(functools.partial(kernel, n_sp, n_dp), out_shape=pltpu.VME...]
where the time goes in v4:
time: 27.3 us; the launch traced here: 27 us
  Pallas kernels  26 us (95%)
  local copies, waits for them, and re-layouts  0.97 us (4%)
    pallas_call x1, Pallas kernels, per_device(): pl.pallas_call(functools.partial(kernel, n_sp, n_dp), out_shape=pltpu.VME...  26 us
    unnamed x1, local copies, waits for them, and re-layouts  0.97 us

profile of v4, /device:TPU:0, one launch (start us, length us, event | category | flops | bytes accessed | tf_op | source)
XLA Modules:
  0.0 27.0 jit_solution(5453413051245888264)
XLA Ops:
  0.0 26.0 %conv_module.1 = bf16[256,2048]{1,0:T(8,128)(2,1)S(1)} custom-call(bf16[2048,256]{1,0:T(8,128)(2,1)} %lin_hbm.1, bf16[2048,256]{1,0:T(8,128)(2,1)} %gate_hbm.1, f32[31,2048]{1,0:T(8,128)} %taps_hbm.1, f32[1,2048]{1,0:T(1,128)} %bitcast.2, f32[1,2048]{1,0:T(1,128)} %bitcast.3, bf16[2048,512]{1,0:T(8,128)(2,1)} %w_hbm.1), custom_call_target="tpu_custom_call" | custom-call | tf_op jit(solution)/shard_map/conv_module/pallas_call | solution.py:423
  26.0 1.0 %copy.8 = bf16[256,2048]{1,0:T(8,128)(2,1)} copy(bf16[256,2048]{1,0:T(8,128)(2,1)S(1)} %conv_module.1) | data formatting | bytes 2097152

commit v5 on v4

--- a/solution.py
+++ b/solution.py
@@ -73,7 +73,13 @@
     def own_piece(n, p):
         return load(w_hbm.at[piece_of(p), :], wbuf.at[d, piece_of(p), :], own_sem.at[n])
 
-    own_loads = [own_piece(0, q)]
+    def own_cut(n, low, high):
+        cut = pl.ds(pl.multiple_of(q * piece + low * rows, rows), (high - low) * rows)
+        return load(w_hbm.at[cut, :], wbuf.at[d, cut, :], own_sem.at[n])
+
+    head = CHUNKS // 8
+    own_head = own_cut(4, 0, head)
+    own_loads = [own_cut(0, head, CHUNKS)]
     in_rows = channels // 4
     loads = []
     for i in range(4):
@@ -101,7 +107,7 @@
     def push(*args):
         copy(*args).start()
 
-    own_loads[0].wait()
+    own_head.wait()
     pl.semaphore_wait(barrier, n_peers)
 
     b_part = list(range(0, BY_X))
@@ -114,6 +120,8 @@
             push(at(d, p, i), at(d, p, i), y_send.at[k - 1], y_recv.at[k - 1, m], target)
 
     for i in range(CHUNKS):
+        if i == head:
+            own_loads[0].wait()
         send_y(q, i, i)
     own_loads[1].wait()
     for n, i in enumerate(a_part):
@@ -441,7 +449,7 @@
                 pltpu.VMEM((2, slabs, PAD, LANES), jnp.bfloat16),
                 dma((2, 4)),
                 dma((3,)),
-                dma((4,)),
+                dma((5,)),
                 dma((2,)),
                 dma((2,)),
                 dma((2,)),

time: 27.3 us -> 27.2 us (level)
  no operation moved by 1% of the time
where the time goes in v5:
time: 27.2 us; the launch traced here: 27 us
  Pallas kernels  26 us (96%)
  local copies, waits for them, and re-layouts  0.97 us (4%)
    pallas_call x1, Pallas kernels, per_device(): pl.pallas_call(functools.partial(kernel, n_sp, n_dp), out_shape=pltpu.VME...  26 us
    unnamed x1, local copies, waits for them, and re-layouts  0.97 us

profile of v5, /device:TPU:0, one launch (start us, length us, event | category | flops | bytes accessed | tf_op | source)
XLA Modules:
  0.0 27.0 jit_solution(17432097058500066711)
XLA Ops:
  0.0 26.0 %conv_module.1 = bf16[256,2048]{1,0:T(8,128)(2,1)S(1)} custom-call(bf16[2048,256]{1,0:T(8,128)(2,1)} %lin_hbm.1, bf16[2048,256]{1,0:T(8,128)(2,1)} %gate_hbm.1, f32[31,2048]{1,0:T(8,128)} %taps_hbm.1, f32[1,2048]{1,0:T(1,128)} %bitcast.2, f32[1,2048]{1,0:T(1,128)} %bitcast.3, bf16[2048,512]{1,0:T(8,128)(2,1)} %w_hbm.1), custom_call_target="tpu_custom_call" | custom-call | tf_op jit(solution)/shard_map/conv_module/pallas_call | solution.py:431
  26.0 1.0 %copy.8 = bf16[256,2048]{1,0:T(8,128)(2,1)} copy(bf16[256,2048]{1,0:T(8,128)(2,1)S(1)} %conv_module.1) | data formatting | bytes 2097152
